TPU v7x, 512 devices: a whole 4x4x16 slice. The times are simulated.
512 devices in a mesh: ep: 128 (over z, x, core), tp: 4 (over y).
Axes of the slice: x: 4, y: 4, z: 16, core: 2. Of those that a mesh axis runs over, the one named last changes fastest.
Arguments:
- tokens: bfloat16 [512, 2048], P('ep', 'tp'), may hold values from -6 to 6
- norm_gain: bfloat16 [2048], P('tp'), may hold values from 0.099609375 to 1.8984375
- w_query: bfloat16 [2048, 2048], P('tp', 'ep'), may hold values from -0.125 to 0.125
- w_forget: bfloat16 [2048, 2048], P('tp', 'ep'), may hold values from -0.125 to 0.125
- w_input: bfloat16 [2048, 2048], P('tp', 'ep'), may hold values from -0.125 to 0.125
- forget_floor: float32 [2048], P('tp'), may hold values from 0 to 0.9
- head_gain: bfloat16 [128], replicated, may hold values from 0.099609375 to 1.8984375
- w_output: bfloat16 [2048, 2048], P('tp', 'ep'), may hold values from -0.125 to 0.125
- state: float32 [512, 16, 128, 128], P('ep', 'tp'), may hold values from -6 to 6
- ffn_gain: bfloat16 [2048], P('tp'), may hold values from 0.099609375 to 1.8984375
- route_experts: int32 [512, 2], P('ep'), may hold values from 0 to 7, all different within a row; in each aligned block of 4 rows (0 to 3, 4 to 7, ...) at most 2 rows name the same one
- route_weights: float32 [512, 2], P('ep'), may hold values from 0.1 to 1
- w_gate: bfloat16 [128, 2048, 448], P('ep', None, 'tp'), may hold values from -0.125 to 0.125
- w_up: bfloat16 [128, 2048, 448], P('ep', None, 'tp'), may hold values from -0.125 to 0.125
- w_down: bfloat16 [128, 448, 2048], P('ep', 'tp'), may hold values from -0.0625 to 0.0625
Outputs:
- mixed: bfloat16 [512, 2048], P('ep', 'tp')
- new_state: float32 [512, 16, 128, 128], P('ep', 'tp')
Inputs may be any that keep to these rules, and one draw needn't show every extreme that they name: `route_experts`: each row names two different experts. Among the rows of one index of ep, no expert is named by more than 2 rows, and in every draw some expert is named by exactly 2 of them.
All inputs are finite; a program needn't handle non-finite values.
Results may differ from a plain program's by a relative error of at most 0.014.
Values may be sent and summed in bfloat16 or wider, within the bound.
No kernel may reach another device: no remote copies, remote signals or barrier semaphores. Data moves between devices by JAX's collectives and lax.ppermute only.
A program may use at most 64 MiB of HBM per device.

v0:
```python
import jax
import jax.numpy as jnp
from jax import lax
from jax.sharding import Mesh
from jax.sharding import PartitionSpec as P

EXPERTS = 8
EP = ("ep_0", "ep_1", "ep_2")
EPS = 1e-06


def laid_out(blocks, dim):
    blocks = jnp.moveaxis(blocks, 0, dim)
    dims = blocks.shape
    return blocks.reshape(*dims[:dim], dims[dim] * dims[dim + 1], *dims[dim + 2 :])


def all_blocks(shard, axes, sequence):
    blocks = shard
    for k in sequence:
        blocks = lax.all_gather(blocks, axes[k])
    done = sequence[::-1]
    back = [done.index(k) for k in range(len(axes))]
    blocks = blocks.transpose(*back, *range(len(axes), blocks.ndim))
    return blocks.reshape(-1, *shard.shape)


def whole_of(shard, axes, sequence, dim):
    return laid_out(all_blocks(shard, axes, sequence), dim)


def in_blocks(shard, dim, length):
    before, after = (shard.shape[:dim], shard.shape[dim + 1 :])
    return jnp.moveaxis(shard.reshape(*before, length, -1, *after), dim, 0)


def sent_and_summed(shard, axis, dim):
    length = lax.axis_size(axis)
    blocks = lax.all_to_all(in_blocks(shard, dim, length), axis, 0, 0, tiled=True)
    return jnp.sum(blocks, axis=0)


def summed_on_arrival(shard, axis, dim):
    blocks = in_blocks(shard, dim, lax.axis_size(axis))
    arrived = lax.all_to_all(blocks, axis, split_axis=0, concat_axis=0, tiled=True)
    return arrived.astype(jnp.float32).sum(axis=0)


def shards(
    tokens,
    norm_gain,
    w_query,
    w_forget,
    w_input,
    forget_floor,
    head_gain,
    w_output,
    state,
    ffn_gain,
    route_experts,
    route_weights,
    w_gate,
    w_up,
    w_down,
):
    ep_count = lax.axis_size(EP)
    tp_count = lax.axis_size("tp")
    seq_count = tokens.shape[0]
    model_width = tokens.shape[1] * tp_count
    head_size = state.shape[2]
    local_heads = state.shape[1]
    tok_f32 = tokens.astype(jnp.float32)
    sum_sq = lax.psum(jnp.sum(tok_f32 * tok_f32, axis=1), "tp")
    normed = (
        tok_f32 * lax.rsqrt(sum_sq / model_width + EPS)[:, None] * norm_gain.astype(jnp.float32)
    ).astype(jnp.bfloat16)
    w_joint = jnp.concatenate([w_query, w_forget, w_input], axis=1)
    partial_value = jnp.dot(
        whole_of(normed, EP, (1, 0, 2), 0), w_joint, preferred_element_type=jnp.float32
    )
    moved_in = lax.all_to_all(partial_value, EP, split_axis=0, concat_axis=1, tiled=True)
    summed = sent_and_summed(moved_in, "tp", 1)
    col_count = w_query.shape[1]
    blocks = summed.reshape(seq_count, -1, 3, col_count)
    queries = blocks[:, :, 0, :].reshape(seq_count, local_heads, head_size)
    fgate = blocks[:, :, 1, :].reshape(seq_count, local_heads, head_size)
    inputs = blocks[:, :, 2, :].reshape(seq_count, local_heads, head_size)
    floors = forget_floor.reshape(local_heads, head_size)
    forget = floors + (1.0 - floors) * jax.nn.sigmoid(fgate)
    new_state = forget[..., None] * state + (1.0 - forget)[..., None] * inputs[:, :, None, :]
    reads = jnp.einsum(
        "bhk,bhkv->bhv", jax.nn.silu(queries), new_state, precision=lax.Precision.HIGHEST
    )
    head_sq = jnp.mean(reads * reads, axis=-1, keepdims=True)
    heads_out = (
        (reads * lax.rsqrt(head_sq + EPS) * head_gain.astype(jnp.float32))
        .reshape(seq_count, local_heads * head_size)
        .astype(jnp.bfloat16)
    )
    part_out = jnp.dot(
        whole_of(heads_out, EP, (1, 0, 2), 0), w_output, preferred_element_type=jnp.float32
    )
    moved_out = lax.all_to_all(
        part_out.astype(jnp.bfloat16), EP, split_axis=0, concat_axis=1, tiled=True
    ).astype(part_out.dtype)
    mixer_slice = summed_on_arrival(moved_out.astype(jnp.bfloat16), "tp", 1).astype(jnp.bfloat16)
    middle = (tok_f32 + mixer_slice.astype(jnp.float32)).astype(jnp.bfloat16)
    middle_f32 = middle.astype(jnp.float32)
    span_count = ep_count // EXPERTS
    capacity = max(2, seq_count // 2)
    positions = jnp.arange(seq_count, dtype=jnp.int32)
    earlier = positions[None, :] < positions[:, None]
    same_expert = route_experts[:, :, None, None] == route_experts[None, None, :, :]
    slot_rank = jnp.sum(same_expert & earlier[:, None, :, None], axis=(2, 3))
    owners = jnp.arange(ep_count, dtype=jnp.int32) // span_count
    matched = route_experts[None, :, :] == owners[:, None, None]
    placed = slot_rank[:, :, None] == jnp.arange(capacity, dtype=jnp.int32)[None, None, :]
    slot_hits = matched[:, :, :, None] & placed[None, :, :, :]
    chosen = jnp.sum(slot_hits.astype(jnp.float32), axis=2).astype(jnp.bfloat16)
    weight_hits = jnp.sum(slot_hits.astype(jnp.float32) * route_weights[None, :, :, None], axis=2)
    row_stat = lax.psum(jnp.sum(middle_f32 * middle_f32, axis=1), "tp")
    second = (
        middle_f32 * lax.rsqrt(row_stat / model_width + EPS)[:, None] * ffn_gain.astype(jnp.float32)
    ).astype(jnp.bfloat16)
    outgoing = jnp.einsum("pts,td->psd", chosen, second, preferred_element_type=jnp.float32).astype(
        jnp.bfloat16
    )
    arrived_part = lax.all_to_all(outgoing, EP, split_axis=0, concat_axis=0, tiled=True)
    arrived = lax.all_gather(arrived_part, "tp", axis=2, tiled=True)
    expert_rows = arrived.reshape(ep_count * capacity, model_width)
    gate_act = jnp.dot(expert_rows, w_gate[0], preferred_element_type=jnp.float32)
    up_act = jnp.dot(expert_rows, w_up[0], preferred_element_type=jnp.float32)
    hidden = (jax.nn.silu(gate_act) * up_act).astype(jnp.bfloat16)
    piece_out = jnp.dot(hidden, w_down[0], preferred_element_type=jnp.float32)
    piece_total = summed_on_arrival(piece_out.astype(jnp.bfloat16), "tp", 1)
    returned = lax.all_to_all(
        piece_total.reshape(ep_count, capacity, -1).astype(jnp.bfloat16),
        EP,
        split_axis=0,
        concat_axis=0,
        tiled=True,
    ).astype(jnp.float32)
    routed = jnp.einsum("pts,psd->td", weight_hits, returned, precision=lax.Precision.HIGHEST)
    result = (middle_f32 + routed).astype(jnp.bfloat16)
    return (result, new_state)


def solution(mesh):
    torus = Mesh(mesh.devices.reshape(16, 4, 2, mesh.shape["tp"]), ("ep_0", "ep_1", "ep_2", "tp"))
    in_specs = (
        P(EP, "tp"),
        P("tp"),
        P("tp", EP),
        P("tp", EP),
        P("tp", EP),
        P("tp"),
        P(),
        P("tp", EP),
        P(EP, "tp", None, None),
        P("tp"),
        P(EP, None),
        P(EP, None),
        P(EP, None, "tp"),
        P(EP, None, "tp"),
        P(EP, "tp", None),
    )
    out_specs = (P(EP, "tp"), P(EP, "tp", None, None))
    return jax.shard_map(
        shards, mesh=torus, in_specs=in_specs, out_specs=out_specs, check_vma=False
    )
```

profile of v0, /device:TPU:33, one launch (start us, length us, event | category | flops | bytes accessed | tf_op | source)
XLA Modules:
  0.0 324.9 jit_solution(1485527307813868062)
XLA Ops:
  7.2 0.9 fusion.22
  8.0 8.7 %psum.14 = f32[4]{0:T(128)S(1)} all-reduce(f32[4]{0:T(128)S(1)} %fusion.22), channel_id=1, replica_groups=mesh['ep_0'=16,'ep_1'=4,'ep_2'=2,'tp'=4] {'tp'}, use_global_device_ids=true, to_apply=%region_1.0 | all-reduce | flops 4 | bytes 32 | tf_op jit(solution)/shard_map/psum | solution.py:73
  16.8 0.7 convert_element_type.76
  17.5 0.8 fusion.31
  18.2 9.5 %all-gather.5 = bf16[4,4,512]{2,1,0:T(4,128)(2,1)S(1)} all-gather(bf16[1,4,512]{2,1,0:T(4,128)(2,1)S(1)} %fusion.31), channel_id=2, replica_groups=mesh['ep_0'=16,'ep_1'=4,'ep_2'=2,'tp'=4] {'ep_1'}, dimensions={0}, use_global_device_ids=true | all-gather | bytes 20480 | tf_op jit(solution)/shard_map/all_gather | solution.py:21
  27.7 27.8 %all-gather.1 = bf16[64,4,512]{2,1,0:T(4,128)(2,1)S(1)} all-gather(bf16[4,4,512]{2,1,0:T(4,128)(2,1)S(1)} %all-gather.5), channel_id=3, replica_groups=mesh['ep_0'=16,'ep_1'=4,'ep_2'=2,'tp'=4] {'ep_0'}, dimensions={0}, use_global_device_ids=true | all-gather | bytes 278528 | tf_op jit(solution)/shard_map/all_gather | solution.py:21
  55.4 14.3 %all-gather.2 = bf16[32,4,4,512]{3,2,1,0:T(4,128)(2,1)S(1)} all-gather(bf16[16,4,4,512]{3,2,1,0:T(4,128)(2,1)S(1)} %bitcast.70), channel_id=4, replica_groups=mesh['ep_0'=16,'ep_1'=4,'ep_2'=2,'tp'=4] {'ep_2'}, dimensions={0}, use_global_device_ids=true | all-gather | bytes 786432 | tf_op jit(solution)/shard_map/all_gather | solution.py:21
  71.3 1.0 reshape.148
  72.2 12.0 %all-to-all-start = ((f32[128,1,192]{2,1,0:T(1,128)}), f32[128,1,192]{2,1,0:T(1,128)S(1)}, u32[]{:S(2)}, u32[]{:S(2)}) async-start(f32[128,1,192]{2,1,0:T(1,128)} %reshape.148), calls=%async_computation | async-start | bytes 262144 | tf_op jit(solution)/shard_map/all_to_all | solution.py:81
  84.4 17.0 %all-to-all-done = f32[128,1,192]{2,1,0:T(1,128)S(1)} async-done(((f32[128,1,192]{2,1,0:T(1,128)}), f32[128,1,192]{2,1,0:T(1,128)S(1)}, u32[]{:S(2)}, u32[]{:S(2)}) %all-to-all-start) | async-done | bytes 98336 | tf_op jit(solution)/shard_map/all_to_all | solution.py:81
  101.9 1.0 reduce.10
  103.3 0.7 copy.124
  103.9 3.3 %all-to-all-start.1 = ((f32[4,4,1536]{2,1,0:T(4,128)}), f32[4,4,1536]{2,1,0:T(4,128)S(1)}, u32[]{:S(2)}, u32[]{:S(2)}) async-start(f32[4,4,1536]{2,1,0:T(4,128)} %copy.124), calls=%async_computation.1 | async-start | bytes 196608 | tf_op jit(solution)/shard_map/all_to_all | solution.py:39
  107.5 4.4 %all-to-all-done.1 = f32[4,4,1536]{2,1,0:T(4,128)S(1)} async-done(((f32[4,4,1536]{2,1,0:T(4,128)}), f32[4,4,1536]{2,1,0:T(4,128)S(1)}, u32[]{:S(2)}, u32[]{:S(2)}) %all-to-all-start.1) | async-done | bytes 98336 | tf_op jit(solution)/shard_map/all_to_all | solution.py:39
  113.6 1.0 copy-done.1
  114.6 1.0 fusion.38
  115.8 9.1 %all_gather.43 = bf16[4,4,512]{2,1,0:T(4,128)(2,1)S(1)} all-gather(bf16[1,4,512]{2,1,0:T(4,128)(2,1)S(1)} %convert_element_type.80), channel_id=1, replica_groups=mesh['ep_0'=16,'ep_1'=4,'ep_2'=2,'tp'=4] {'ep_1'}, dimensions={0}, use_global_device_ids=true | all-gather | bytes 20480 | tf_op jit(solution)/shard_map/all_gather | solution.py:21
  124.9 20.2 %all-gather.3 = bf16[64,4,512]{2,1,0:T(4,128)(2,1)S(1)} all-gather(bf16[4,4,512]{2,1,0:T(4,128)(2,1)S(1)} %all_gather.43), channel_id=5, replica_groups=mesh['ep_0'=16,'ep_1'=4,'ep_2'=2,'tp'=4] {'ep_0'}, dimensions={0}, use_global_device_ids=true | all-gather | bytes 278528 | tf_op jit(solution)/shard_map/all_gather | solution.py:21
  145.1 13.3 %all-gather.4 = bf16[32,4,4,512]{3,2,1,0:T(4,128)(2,1)S(1)} all-gather(bf16[16,4,4,512]{3,2,1,0:T(4,128)(2,1)S(1)} %bitcast.71), channel_id=6, replica_groups=mesh['ep_0'=16,'ep_1'=4,'ep_2'=2,'tp'=4] {'ep_2'}, dimensions={0}, use_global_device_ids=true | all-gather | bytes 786432 | tf_op jit(solution)/shard_map/all_gather | solution.py:21
  159.7 0.8 copy.129
  160.4 9.0 %all-to-all-start.2 = ((bf16[128,4,16]{2,1,0:T(4,128)(2,1)}), bf16[128,4,16]{2,1,0:T(4,128)(2,1)S(1)}, u32[]{:S(2)}, u32[]{:S(2)}) async-start(bf16[128,4,16]{2,1,0:T(4,128)(2,1)} %bitcast.15), calls=%async_computation.2 | async-start | bytes 262144 | tf_op jit(solution)/shard_map/all_to_all | solution.py:103
  169.5 17.1 %all-to-all-done.2 = bf16[128,4,16]{2,1,0:T(4,128)(2,1)S(1)} async-done(((bf16[128,4,16]{2,1,0:T(4,128)(2,1)}), bf16[128,4,16]{2,1,0:T(4,128)(2,1)S(1)}, u32[]{:S(2)}, u32[]{:S(2)}) %all-to-all-start.2) | async-done | bytes 16416 | tf_op jit(solution)/shard_map/all_to_all | solution.py:103
  187.3 3.2 all-to-all-start.3
  190.7 4.0 %all-to-all-done.3 = bf16[4,4,512]{2,1,0:T(4,128)(2,1)S(1)} async-done(((bf16[4,4,512]{2,1,0:T(4,128)(2,1)}), bf16[4,4,512]{2,1,0:T(4,128)(2,1)S(1)}, u32[]{:S(2)}, u32[]{:S(2)}) %all-to-all-start.3) | async-done | bytes 16416 | tf_op jit(solution)/shard_map/all_to_all | solution.py:45
  194.9 6.9 %psum.15 = f32[4]{0:T(128)S(1)} all-reduce(f32[4]{0:T(128)S(1)} %fusion.26), channel_id=1, replica_groups=mesh['ep_0'=16,'ep_1'=4,'ep_2'=2,'tp'=4] {'tp'}, use_global_device_ids=true, to_apply=%region_9.10 | all-reduce | flops 4 | bytes 32 | tf_op jit(solution)/shard_map/psum | solution.py:121
  202.4 31.9 %all_to_all.54 = bf16[128,2,512]{2,1,0:T(2,128)(2,1)} all-to-all(bf16[128,2,512]{2,1,0:T(2,128)(2,1)S(1)} %copy.132), channel_id=1, replica_groups=mesh['ep_0'=16,'ep_1'=4,'ep_2'=2,'tp'=4] {'ep_0','ep_1','ep_2'}, dimensions={0} | all-to-all | bytes 524288 | tf_op jit(solution)/shard_map/all_to_all | solution.py:128
  234.4 20.6 %all-gather.8.cloned.1.call-done = bf16[128,2,2048]{2,1,0:T(2,128)(2,1)} async-done(((bf16[128,2,512]{2,1,0:T(2,128)(2,1)}), bf16[128,2,2048]{2,1,0:T(2,128)(2,1)}) %all-gather.8.cloned.1.call-update) | async-done | bytes 1048592 | tf_op jit(solution)/shard_map/all_gather | solution.py:129
  255.0 1.5 reshape.121
  257.5 1.4 convolution_convert_fusion
  259.0 16.2 %all_to_all.55 = bf16[4,256,512]{2,1,0:T(8,128)(2,1)S(1)} all-to-all(bf16[4,256,512]{2,1,0:T(8,128)(2,1)S(1)} %bitcast.67), channel_id=1, replica_groups=mesh['ep_0'=16,'ep_1'=4,'ep_2'=2,'tp'=4] {'tp'}, dimensions={0} | all-to-all | bytes 2097152 | tf_op jit(solution)/shard_map/all_to_all | solution.py:45
  275.5 41.7 %all_to_all.56 = bf16[128,2,512]{2,1,0:T(2,128)(2,1)S(1)} all-to-all(bf16[128,2,512]{2,1,0:T(2,128)(2,1)S(1)} %convert_element_type.93), channel_id=1, replica_groups=mesh['ep_0'=16,'ep_1'=4,'ep_2'=2,'tp'=4] {'ep_0','ep_1','ep_2'}, dimensions={0} | all-to-all | bytes 524288 | tf_op jit(solution)/shard_map/all_to_all | solution.py:136
  317.2 0.8 fusion.2
  (82 shorter events, 8.9 us)
Async XLA Ops:
  7.2 249.8 %copy-start = (bf16[1,112,2048]{2,1,0:T(8,128)(2,1)S(1)}, bf16[1,112,2048]{2,1,0:T(8,128)(2,1)}, u32[]{:S(2)}) copy-start(bf16[1,112,2048]{2,1,0:T(8,128)(2,1)} %param.29) | copy-start | bytes 1376260
  70.0 0.8 copy-start.7
  70.0 0.8 copy-start.8
  70.0 0.8 copy-start.9
  70.8 13.4 %copy-start.10 = (s32[4,2]{0,1:T(2,128)S(1)}, s32[4,2]{0,1:T(2,128)}, u32[]{:S(2)}) copy-start(s32[4,2]{0,1:T(2,128)} %param.25) | copy-start | bytes 100
  70.8 13.5 %copy-start.14 = (bf16[128]{0:T(256)(128)(2,1)S(1)}, bf16[128]{0:T(256)(128)(2,1)}, u32[]{:S(2)}) copy-start(bf16[128]{0:T(256)(128)(2,1)} %param.21) | copy-start | bytes 772
  70.9 13.5 %copy-start.11 = (f32[512]{0:T(512)S(1)}, f32[512]{0:T(512)}, u32[]{:S(2)}) copy-start(f32[512]{0:T(512)} %param.20) | copy-start | bytes 6148
  72.2 29.1 %all-to-all-start = ((f32[128,1,192]{2,1,0:T(1,128)}), f32[128,1,192]{2,1,0:T(1,128)S(1)}, u32[]{:S(2)}, u32[]{:S(2)}) async-start(f32[128,1,192]{2,1,0:T(1,128)} %reshape.148), calls=%async_computation | async-start | bytes 262144 | tf_op jit(solution)/shard_map/all_to_all | solution.py:81
  103.0 10.0 %copy-start.2 = (f32[4,4,128,128]{3,2,1,0:T(8,128)S(1)}, f32[4,4,128,128]{3,2,1,0:T(8,128)}, u32[]{:S(2)}) copy-start(f32[4,4,128,128]{3,2,1,0:T(8,128)} %param.23) | copy-start | bytes 3145732
  103.9 7.9 %all-to-all-start.1 = ((f32[4,4,1536]{2,1,0:T(4,128)}), f32[4,4,1536]{2,1,0:T(4,128)S(1)}, u32[]{:S(2)}, u32[]{:S(2)}) async-start(f32[4,4,1536]{2,1,0:T(4,128)} %copy.124), calls=%async_computation.1 | async-start | bytes 196608 | tf_op jit(solution)/shard_map/all_to_all | solution.py:39
  113.6 1.0 copy-start.1
  158.7 0.7 copy-start.6
  159.1 31.5 %copy-start.12 = (f32[4,2]{0,1:T(2,128)S(1)}, f32[4,2]{0,1:T(2,128)}, u32[]{:S(2)}) copy-start(f32[4,2]{0,1:T(2,128)} %param.26) | copy-start | bytes 100
  159.1 35.6 %copy-start.5 = (bf16[4,512]{1,0:T(4,128)(2,1)S(1)}, bf16[4,512]{1,0:T(4,128)(2,1)}, u32[]{:S(2)}) copy-start(bf16[4,512]{1,0:T(4,128)(2,1)} %param.15) | copy-start | bytes 12292
  159.2 35.8 %copy-start.13 = (bf16[512]{0:T(512)(128)(2,1)S(1)}, bf16[512]{0:T(512)(128)(2,1)}, u32[]{:S(2)}) copy-start(bf16[512]{0:T(512)(128)(2,1)} %param.24) | copy-start | bytes 3076
  160.4 26.1 %all-to-all-start.2 = ((bf16[128,4,16]{2,1,0:T(4,128)(2,1)}), bf16[128,4,16]{2,1,0:T(4,128)(2,1)S(1)}, u32[]{:S(2)}, u32[]{:S(2)}) async-start(bf16[128,4,16]{2,1,0:T(4,128)(2,1)} %bitcast.15), calls=%async_computation.2 | async-start | bytes 262144 | tf_op jit(solution)/shard_map/all_to_all | solution.py:103
  187.3 7.4 %all-to-all-start.3 = ((bf16[4,4,512]{2,1,0:T(4,128)(2,1)}), bf16[4,4,512]{2,1,0:T(4,128)(2,1)S(1)}, u32[]{:S(2)}, u32[]{:S(2)}) async-start(bf16[4,4,512]{2,1,0:T(4,128)(2,1)} %copy.131), calls=%async_computation.3 | async-start | bytes 32768 | tf_op jit(solution)/shard_map/all_to_all | solution.py:45
  190.6 64.4 %all-gather.8.cloned.1.call-start = ((), (), s32[]{:S(2)}) async-start(), calls=%async_computation.7 | async-start | bytes 1310720 | tf_op jit(solution)/shard_map/all_gather | solution.py:129
  234.4 22.1 %copy-start.4 = (bf16[1,2048,112]{1,2,0:T(8,128)(2,1)S(1)}, bf16[1,2048,112]{1,2,0:T(8,128)(2,1)}, u32[]{:S(2)}) copy-start(bf16[1,2048,112]{1,2,0:T(8,128)(2,1)} %param.27) | copy-start | bytes 1376260
  256.4 1.0 copy-start.3
Sparse Core Ops, SparseCore 0:
  234.5 20.4 all-gather.7
where the time goes:
time: 326 us; the launch traced here: 325 us
  blocking collectives  200 us (61%)
  waiting for transfers between devices  63.1 us (19%)
  starting transfers between devices  27.6 us (8%)
  between operations  14.5 us (4%)
  local copies, waits for them, and re-layouts  10.8 us (3%)
  other arithmetic  4.91 us (2%)
  matrix products  4.43 us (1%)
    all_gather x6, blocking collectives, all_blocks(): blocks = lax.all_gather(blocks, axes[k])  94.2 us
    all_to_all x1, blocking collectives, shards(): lax.all_to_all(piece_total.reshape(ep_count, capacity, -1).astype(jnp.bfl...  41.7 us
    all_to_all x1, blocking collectives, shards(): lax.all_to_all(outgoing, EP, split_axis=0, concat_axis=0, tiled=True)  31.9 us
    all_gather x1, waiting for transfers between devices, shards(): arrived = lax.all_gather(arrived_part, 'tp', axis=2, tiled=True)  20.6 us
    all_to_all x1, waiting for transfers between devices, shards(): lax.all_to_all(part_out.astype(jnp.bfloat16), EP, split_axis=0, concat_ax...  17.1 us
    all_to_all x1, waiting for transfers between devices, shards(): lax.all_to_all(partial_value, EP, split_axis=0, concat_axis=1, tiled=True)  17 us
    all_to_all x1, blocking collectives, summed_on_arrival(): lax.all_to_all(blocks, axis, split_axis=0, concat_axis=0, tiled=True)  16.2 us
    all_to_all x1, starting transfers between devices, shards(): lax.all_to_all(partial_value, EP, split_axis=0, concat_axis=1, tiled=True)  12 us
  transfers between devices with their start and end apart: 5, of which 5 were waited for; matrix products, arithmetic and copies ran while one was open for 0% of the time, Pallas kernels for 0%

commit v1 on v0

--- a/solution.py
+++ b/solution.py
@@ -126,7 +126,11 @@
         jnp.bfloat16
     )
     arrived_part = lax.all_to_all(outgoing, EP, split_axis=0, concat_axis=0, tiled=True)
-    arrived = lax.all_gather(arrived_part, "tp", axis=2, tiled=True)
+    size = lax.axis_size("tp")
+    repeats = [size if d == 2 else 1 for d in range(arrived_part.ndim)]
+    arrived = lax.all_to_all(
+        jnp.tile(arrived_part, repeats), "tp", split_axis=2, concat_axis=2, tiled=True
+    )
     expert_rows = arrived.reshape(ep_count * capacity, model_width)
     gate_act = jnp.dot(expert_rows, w_gate[0], preferred_element_type=jnp.float32)
     up_act = jnp.dot(expert_rows, w_up[0], preferred_element_type=jnp.float32)

time: 326 us -> 301 us (0.923)
  waiting for transfers between devices: 63.1 us -> 42.5 us
  between operations: 14.5 us -> 1.12 us
  blocking collectives: 200 us -> 205 us
    all_gather x1 -> x0, waiting for transfers between devices: 20.6 us -> none  [shards(): arrived = lax.all_gather(arrived_part, 'tp', axis=2, tiled=True)]
    all_to_all x0 -> x1, blocking collectives: none -> 17.3 us  [shards(): lax.all_to_all(jnp.tile(arrived_part, repeats), 'tp', split_axis=2, conca...]
    all_to_all x1, blocking collectives: 41.7 us -> 29.9 us  [shards(): lax.all_to_all(piece_total.reshape(ep_count, capacity, -1).astype(jnp.bfl...]
    all_to_all x0 -> x2, local copies, waits for them, and re-layouts: none -> 3.4 us  [the longest x1 3.01 us: shards(): lax.all_to_all(jnp.tile(arrived_part, repeats), 'tp', split_axis=2, conca...]
  transfers between devices with their start and end apart: 5 -> 4, of which waited for: 5 -> 4; matrix products, arithmetic and copies ran while one was open for 0% -> 0% of each run, Pallas kernels for 0% -> 0%
where the time goes in v1:
time: 301 us; the launch traced here: 300 us
  blocking collectives  205 us (68%)
  waiting for transfers between devices  42.5 us (14%)
  starting transfers between devices  27.6 us (9%)
  local copies, waits for them, and re-layouts  13.2 us (4%)
  matrix products  5.51 us (2%)
  other arithmetic  4.91 us (2%)
    all_gather x6, blocking collectives, all_blocks(): blocks = lax.all_gather(blocks, axes[k])  94.2 us
    all_to_all x1, blocking collectives, shards(): lax.all_to_all(outgoing, EP, split_axis=0, concat_axis=0, tiled=True)  31.8 us
    all_to_all x1, blocking collectives, shards(): lax.all_to_all(piece_total.reshape(ep_count, capacity, -1).astype(jnp.bfl...  29.9 us
    all_to_all x1, blocking collectives, shards(): lax.all_to_all(jnp.tile(arrived_part, repeats), 'tp', split_axis=2, conca...  17.3 us
    all_to_all x1, waiting for transfers between devices, shards(): lax.all_to_all(part_out.astype(jnp.bfloat16), EP, split_axis=0, concat_ax...  17.1 us
    all_to_all x1, waiting for transfers between devices, shards(): lax.all_to_all(partial_value, EP, split_axis=0, concat_axis=1, tiled=True)  17 us
    all_to_all x1, blocking collectives, summed_on_arrival(): lax.all_to_all(blocks, axis, split_axis=0, concat_axis=0, tiled=True)  16.4 us
    all_to_all x1, starting transfers between devices, shards(): lax.all_to_all(partial_value, EP, split_axis=0, concat_axis=1, tiled=True)  12 us
  transfers between devices with their start and end apart: 4, of which 4 were waited for; matrix products, arithmetic and copies ran while one was open for 0% of the time, Pallas kernels for 0%

profile of v1, /device:TPU:33, one launch (start us, length us, event | category | flops | bytes accessed | tf_op | source)
XLA Modules:
  0.0 300.0 jit_solution(13555992844682213496)
XLA Ops:
  0.6 0.9 fusion.22
  1.5 8.7 %psum.14 = f32[4]{0:T(128)S(1)} all-reduce(f32[4]{0:T(128)S(1)} %fusion.22), channel_id=1, replica_groups=mesh['ep_0'=16,'ep_1'=4,'ep_2'=2,'tp'=4] {'tp'}, use_global_device_ids=true, to_apply=%region_1.0 | all-reduce | flops 4 | bytes 32 | tf_op jit(solution)/shard_map/psum | solution.py:73
  10.2 0.7 convert_element_type.76
  10.9 0.8 fusion.31
  11.7 9.5 %all-gather.5 = bf16[4,4,512]{2,1,0:T(4,128)(2,1)S(1)} all-gather(bf16[1,4,512]{2,1,0:T(4,128)(2,1)S(1)} %fusion.31), channel_id=2, replica_groups=mesh['ep_0'=16,'ep_1'=4,'ep_2'=2,'tp'=4] {'ep_1'}, dimensions={0}, use_global_device_ids=true | all-gather | bytes 20480 | tf_op jit(solution)/shard_map/all_gather | solution.py:21
  21.1 27.8 %all-gather.1 = bf16[64,4,512]{2,1,0:T(4,128)(2,1)S(1)} all-gather(bf16[4,4,512]{2,1,0:T(4,128)(2,1)S(1)} %all-gather.5), channel_id=3, replica_groups=mesh['ep_0'=16,'ep_1'=4,'ep_2'=2,'tp'=4] {'ep_0'}, dimensions={0}, use_global_device_ids=true | all-gather | bytes 278528 | tf_op jit(solution)/shard_map/all_gather | solution.py:21
  48.9 14.3 %all-gather.2 = bf16[32,4,4,512]{3,2,1,0:T(4,128)(2,1)S(1)} all-gather(bf16[16,4,4,512]{3,2,1,0:T(4,128)(2,1)S(1)} %bitcast.72), channel_id=4, replica_groups=mesh['ep_0'=16,'ep_1'=4,'ep_2'=2,'tp'=4] {'ep_2'}, dimensions={0}, use_global_device_ids=true | all-gather | bytes 786432 | tf_op jit(solution)/shard_map/all_gather | solution.py:21
  64.8 1.0 reshape.152
  65.7 12.0 %all-to-all-start = ((f32[128,1,192]{2,1,0:T(1,128)}), f32[128,1,192]{2,1,0:T(1,128)S(1)}, u32[]{:S(2)}, u32[]{:S(2)}) async-start(f32[128,1,192]{2,1,0:T(1,128)} %reshape.152), calls=%async_computation | async-start | bytes 262144 | tf_op jit(solution)/shard_map/all_to_all | solution.py:81
  77.9 17.0 %all-to-all-done = f32[128,1,192]{2,1,0:T(1,128)S(1)} async-done(((f32[128,1,192]{2,1,0:T(1,128)}), f32[128,1,192]{2,1,0:T(1,128)S(1)}, u32[]{:S(2)}, u32[]{:S(2)}) %all-to-all-start) | async-done | bytes 98336 | tf_op jit(solution)/shard_map/all_to_all | solution.py:81
  95.3 1.0 reduce.10
  97.4 3.3 %all-to-all-start.1 = ((f32[4,4,1536]{2,1,0:T(4,128)}), f32[4,4,1536]{2,1,0:T(4,128)S(1)}, u32[]{:S(2)}, u32[]{:S(2)}) async-start(f32[4,4,1536]{2,1,0:T(4,128)} %copy.132), calls=%async_computation.1 | async-start | bytes 196608 | tf_op jit(solution)/shard_map/all_to_all | solution.py:39
  100.9 4.4 %all-to-all-done.1 = f32[4,4,1536]{2,1,0:T(4,128)S(1)} async-done(((f32[4,4,1536]{2,1,0:T(4,128)}), f32[4,4,1536]{2,1,0:T(4,128)S(1)}, u32[]{:S(2)}, u32[]{:S(2)}) %all-to-all-start.1) | async-done | bytes 98336 | tf_op jit(solution)/shard_map/all_to_all | solution.py:39
  107.1 1.0 copy-done.1
  108.1 1.0 fusion.38
  109.2 9.1 %all_gather.40 = bf16[4,4,512]{2,1,0:T(4,128)(2,1)S(1)} all-gather(bf16[1,4,512]{2,1,0:T(4,128)(2,1)S(1)} %convert_element_type.80), channel_id=1, replica_groups=mesh['ep_0'=16,'ep_1'=4,'ep_2'=2,'tp'=4] {'ep_1'}, dimensions={0}, use_global_device_ids=true | all-gather | bytes 20480 | tf_op jit(solution)/shard_map/all_gather | solution.py:21
  118.4 20.2 %all-gather.3 = bf16[64,4,512]{2,1,0:T(4,128)(2,1)S(1)} all-gather(bf16[4,4,512]{2,1,0:T(4,128)(2,1)S(1)} %all_gather.40), channel_id=5, replica_groups=mesh['ep_0'=16,'ep_1'=4,'ep_2'=2,'tp'=4] {'ep_0'}, dimensions={0}, use_global_device_ids=true | all-gather | bytes 278528 | tf_op jit(solution)/shard_map/all_gather | solution.py:21
  138.6 13.3 %all-gather.4 = bf16[32,4,4,512]{3,2,1,0:T(4,128)(2,1)S(1)} all-gather(bf16[16,4,4,512]{3,2,1,0:T(4,128)(2,1)S(1)} %bitcast.73), channel_id=6, replica_groups=mesh['ep_0'=16,'ep_1'=4,'ep_2'=2,'tp'=4] {'ep_2'}, dimensions={0}, use_global_device_ids=true | all-gather | bytes 786432 | tf_op jit(solution)/shard_map/all_gather | solution.py:21
  153.1 0.8 copy.137
  153.9 9.0 %all-to-all-start.2 = ((bf16[128,4,16]{2,1,0:T(4,128)(2,1)}), bf16[128,4,16]{2,1,0:T(4,128)(2,1)S(1)}, u32[]{:S(2)}, u32[]{:S(2)}) async-start(bf16[128,4,16]{2,1,0:T(4,128)(2,1)} %bitcast.15), calls=%async_computation.2 | async-start | bytes 262144 | tf_op jit(solution)/shard_map/all_to_all | solution.py:103
  162.9 17.1 %all-to-all-done.2 = bf16[128,4,16]{2,1,0:T(4,128)(2,1)S(1)} async-done(((bf16[128,4,16]{2,1,0:T(4,128)(2,1)}), bf16[128,4,16]{2,1,0:T(4,128)(2,1)S(1)}, u32[]{:S(2)}, u32[]{:S(2)}) %all-to-all-start.2) | async-done | bytes 16416 | tf_op jit(solution)/shard_map/all_to_all | solution.py:103
  180.8 3.2 %all-to-all-start.3 = ((bf16[4,4,512]{2,1,0:T(4,128)(2,1)}), bf16[4,4,512]{2,1,0:T(4,128)(2,1)S(1)}, u32[]{:S(2)}, u32[]{:S(2)}) async-start(bf16[4,4,512]{2,1,0:T(4,128)(2,1)} %copy.139), calls=%async_computation.3 | async-start | bytes 32768 | tf_op jit(solution)/shard_map/all_to_all | solution.py:45
  184.2 4.1 %all-to-all-done.3 = bf16[4,4,512]{2,1,0:T(4,128)(2,1)S(1)} async-done(((bf16[4,4,512]{2,1,0:T(4,128)(2,1)}), bf16[4,4,512]{2,1,0:T(4,128)(2,1)S(1)}, u32[]{:S(2)}, u32[]{:S(2)}) %all-to-all-start.3) | async-done | bytes 16416 | tf_op jit(solution)/shard_map/all_to_all | solution.py:45
  188.4 6.9 %psum.15 = f32[4]{0:T(128)S(1)} all-reduce(f32[4]{0:T(128)S(1)} %fusion.26), channel_id=1, replica_groups=mesh['ep_0'=16,'ep_1'=4,'ep_2'=2,'tp'=4] {'tp'}, use_global_device_ids=true, to_apply=%region_9.10 | all-reduce | flops 4 | bytes 32 | tf_op jit(solution)/shard_map/psum | solution.py:121
  195.9 31.8 %all_to_all.59 = bf16[128,2,512]{2,1,0:T(2,128)(2,1)S(1)} all-to-all(bf16[128,2,512]{2,1,0:T(2,128)(2,1)S(1)} %copy.140), channel_id=1, replica_groups=mesh['ep_0'=16,'ep_1'=4,'ep_2'=2,'tp'=4] {'ep_0','ep_1','ep_2'}, dimensions={0} | all-to-all | bytes 524288 | tf_op jit(solution)/shard_map/all_to_all | solution.py:128
  228.6 17.3 %all_to_all.60 = bf16[128,2,2048]{0,1,2:T(2,128)(2,1)S(1)} all-to-all(bf16[128,2,2048]{0,1,2:T(2,128)(2,1)S(1)} %bitcast.68), channel_id=1, replica_groups=mesh['ep_0'=16,'ep_1'=4,'ep_2'=2,'tp'=4] {'tp'}, dimensions={2} | all-to-all | bytes 2097152 | tf_op jit(solution)/shard_map/all_to_all | solution.py:131
  245.9 3.0 %copy.142 = bf16[128,2,2048]{2,1,0:T(2,128)(2,1)S(1)} copy(bf16[128,2,2048]{0,1,2:T(2,128)(2,1)S(1)} %all_to_all.60) | data formatting | bytes 2097152 | tf_op jit(solution)/shard_map/all_to_all | solution.py:131
  249.4 1.5 fusion.6
  251.0 1.4 convolution_convert_fusion
  252.5 16.4 %all_to_all.61 = bf16[4,256,512]{2,1,0:T(8,128)(2,1)S(1)} all-to-all(bf16[4,256,512]{2,1,0:T(8,128)(2,1)S(1)} %bitcast.69), channel_id=1, replica_groups=mesh['ep_0'=16,'ep_1'=4,'ep_2'=2,'tp'=4] {'tp'}, dimensions={0} | all-to-all | bytes 2097152 | tf_op jit(solution)/shard_map/all_to_all | solution.py:45
  269.3 29.9 %all_to_all.62 = bf16[128,2,512]{2,1,0:T(2,128)(2,1)S(1)} all-to-all(bf16[128,2,512]{2,1,0:T(2,128)(2,1)S(1)} %convert_element_type.93), channel_id=1, replica_groups=mesh['ep_0'=16,'ep_1'=4,'ep_2'=2,'tp'=4] {'ep_0','ep_1','ep_2'}, dimensions={0} | all-to-all | bytes 524288 | tf_op jit(solution)/shard_map/all_to_all | solution.py:140
  299.2 0.8 fusion.2
  (81 shorter events, 9.9 us)
Async XLA Ops:
  0.6 250.3 %copy-start = (bf16[1,112,2048]{2,1,0:T(8,128)(2,1)S(1)}, bf16[1,112,2048]{2,1,0:T(8,128)(2,1)}, u32[]{:S(2)}) copy-start(bf16[1,112,2048]{2,1,0:T(8,128)(2,1)} %param.29) | copy-start | bytes 1376260
  63.5 0.8 copy-start.6
  63.5 0.8 copy-start.7
  63.5 0.8 copy-start.8
  64.3 13.4 %copy-start.9 = (s32[4,2]{0,1:T(2,128)S(1)}, s32[4,2]{0,1:T(2,128)}, u32[]{:S(2)}) copy-start(s32[4,2]{0,1:T(2,128)} %param.25) | copy-start | bytes 100
  64.3 13.5 %copy-start.13 = (bf16[128]{0:T(256)(128)(2,1)S(1)}, bf16[128]{0:T(256)(128)(2,1)}, u32[]{:S(2)}) copy-start(bf16[128]{0:T(256)(128)(2,1)} %param.21) | copy-start | bytes 772
  64.3 13.5 %copy-start.10 = (f32[512]{0:T(512)S(1)}, f32[512]{0:T(512)}, u32[]{:S(2)}) copy-start(f32[512]{0:T(512)} %param.20) | copy-start | bytes 6148
  65.7 29.1 %all-to-all-start = ((f32[128,1,192]{2,1,0:T(1,128)}), f32[128,1,192]{2,1,0:T(1,128)S(1)}, u32[]{:S(2)}, u32[]{:S(2)}) async-start(f32[128,1,192]{2,1,0:T(1,128)} %reshape.152), calls=%async_computation | async-start | bytes 262144 | tf_op jit(solution)/shard_map/all_to_all | solution.py:81
  96.5 10.0 %copy-start.2 = (f32[4,4,128,128]{3,2,1,0:T(8,128)S(1)}, f32[4,4,128,128]{3,2,1,0:T(8,128)}, u32[]{:S(2)}) copy-start(f32[4,4,128,128]{3,2,1,0:T(8,128)} %param.23) | copy-start | bytes 3145732
  97.4 7.9 %all-to-all-start.1 = ((f32[4,4,1536]{2,1,0:T(4,128)}), f32[4,4,1536]{2,1,0:T(4,128)S(1)}, u32[]{:S(2)}, u32[]{:S(2)}) async-start(f32[4,4,1536]{2,1,0:T(4,128)} %copy.132), calls=%async_computation.1 | async-start | bytes 196608 | tf_op jit(solution)/shard_map/all_to_all | solution.py:39
  107.1 1.0 copy-start.1
  152.2 0.7 copy-start.5
  152.6 31.5 %copy-start.11 = (f32[4,2]{0,1:T(2,128)S(1)}, f32[4,2]{0,1:T(2,128)}, u32[]{:S(2)}) copy-start(f32[4,2]{0,1:T(2,128)} %param.26) | copy-start | bytes 100
  152.6 35.6 %copy-start.4 = (bf16[4,512]{1,0:T(4,128)(2,1)S(1)}, bf16[4,512]{1,0:T(4,128)(2,1)}, u32[]{:S(2)}) copy-start(bf16[4,512]{1,0:T(4,128)(2,1)} %param.15) | copy-start | bytes 12292
  152.6 35.8 %copy-start.12 = (bf16[512]{0:T(512)(128)(2,1)S(1)}, bf16[512]{0:T(512)(128)(2,1)}, u32[]{:S(2)}) copy-start(bf16[512]{0:T(512)(128)(2,1)} %param.24) | copy-start | bytes 3076
  153.9 26.1 %all-to-all-start.2 = ((bf16[128,4,16]{2,1,0:T(4,128)(2,1)}), bf16[128,4,16]{2,1,0:T(4,128)(2,1)S(1)}, u32[]{:S(2)}, u32[]{:S(2)}) async-start(bf16[128,4,16]{2,1,0:T(4,128)(2,1)} %bitcast.15), calls=%async_computation.2 | async-start | bytes 262144 | tf_op jit(solution)/shard_map/all_to_all | solution.py:103
  180.8 7.4 %all-to-all-start.3 = ((bf16[4,4,512]{2,1,0:T(4,128)(2,1)}), bf16[4,4,512]{2,1,0:T(4,128)(2,1)S(1)}, u32[]{:S(2)}, u32[]{:S(2)}) async-start(bf16[4,4,512]{2,1,0:T(4,128)(2,1)} %copy.139), calls=%async_computation.3 | async-start | bytes 32768 | tf_op jit(solution)/shard_map/all_to_all | solution.py:45
  249.4 1.6 copy-start.3
